TPU v7x, 32 devices: a whole 2x2x4 slice. The times are simulated.
32 devices in a mesh: sp: 8 (over z, y), tp: 4 (over x, core).
Axes of the slice: x: 2, y: 2, z: 4, core: 2. Of those that a mesh axis runs over, the one named last changes fastest.
Arguments:
- tokens: bfloat16 [6144, 4096], P('sp', 'tp'), may hold values from -6 to 6
- in_proj: bfloat16 [3, 4096, 1024], P(None, 'tp', 'sp'), may hold values from -0.09375 to 0.09375
- group_mix: bfloat16 [3, 4, 256, 256], replicated, may hold values from -0.375 to 0.375
- pool_gain: float32 [3, 1024], replicated, may hold values from 0.1 to 1.9
- out_proj: bfloat16 [3, 1024, 4096], P(None, 'sp', 'tp'), may hold values from -0.1875 to 0.1875
- norm_gain: float32 [3, 4096], P(None, 'tp'), may hold values from 0.25 to 3
- norm_bias: float32 [3, 4096], P(None, 'tp'), may hold values from -1.5 to 1.5
Outputs:
- stream_out: bfloat16 [6144, 4096], P('sp', 'tp')
All inputs are finite; a program needn't handle non-finite values.
Results may differ from a plain program's by a relative error of at most 0.017.
Values may be sent and summed in bfloat16 or wider, within the bound.
A program may use at most 128 MiB of HBM per device.

v0:
```python
import jax
import jax.numpy as jnp
from jax import lax
from jax.sharding import PartitionSpec as P

pool_windows = (2, 4, 8, 16)
norm_eps = 1e-05


def padded(array, sides, width):
    for axis, dim in sides:
        devices, length = (lax.axis_size(axis), array.shape[dim])
        up = [(i, (i + 1) % devices) for i in range(devices - 1)]
        down = [(j, i) for i, j in up]
        last = lax.slice_in_dim(array, length - width, length, axis=dim)
        leading = lax.slice_in_dim(array, 0, width, axis=dim)
        before = lax.ppermute(last, axis, up)
        after = lax.ppermute(leading, axis, down)
        array = jnp.concatenate([before, array, after], axis=dim)
    return array


def on_device(tokens, in_proj, group_mix, pool_gain, out_proj, norm_gain, norm_bias):
    rows_dev = tokens.shape[0]
    feat_dev = tokens.shape[1]
    layer_count = in_proj.shape[0]
    pool_width = in_proj.shape[2] * lax.axis_size("sp")
    chan_share = pool_width // lax.axis_size("tp")
    group_width = group_mix.shape[2]
    model_width = feat_dev * lax.axis_size("tp")
    residual_scale = (2.0 * layer_count) ** 0.25
    fringe_width = max(pool_windows) // 2
    seq_length = rows_dev * lax.axis_size("sp")
    positions = lax.axis_index("sp") * rows_dev + jnp.arange(rows_dev)
    chan_groups = (lax.axis_index("tp") * chan_share + jnp.arange(chan_share)) // group_width
    in_all, out_all = (
        lax.all_gather(in_proj, "sp", axis=2, tiled=True),
        lax.all_gather(out_proj, "sp", axis=1, tiled=True),
    )
    stream = tokens
    for layer_idx in range(layer_count):
        in_block = in_all[layer_idx]
        out_block = out_all[layer_idx]
        projected = lax.psum_scatter(
            lax.dot_general(
                in_block, stream, (((0,), (1,)), ((), ())), preferred_element_type=jnp.float32
            ).astype(jnp.bfloat16),
            "tp",
            scatter_dimension=0,
            tiled=True,
        )
        extended = padded(projected, (("sp", 1),), fringe_width)
        ext_float = extended.astype(jnp.float32)
        pooled = jnp.zeros((chan_share, rows_dev), jnp.float32)
        for group_idx in range(4):
            own_rows = (chan_groups == group_idx)[:, None]
            span_len = pool_windows[group_idx]
            before = span_len // 2
            after = span_len - before
            window_total = jnp.zeros((ext_float.shape[0], rows_dev), jnp.float32)
            for offset in range(-before, after):
                window_total = (
                    window_total
                    + ext_float[:, fringe_width + offset : fringe_width + offset + rows_dev]
                )
            low_edge = jnp.clip(positions - before, 0, seq_length)
            high_edge = jnp.clip(positions + after, 0, seq_length)
            pooled = jnp.where(
                own_rows, window_total / (high_edge - low_edge).astype(jnp.float32)[None, :], pooled
            )
        differ = (pooled - projected.astype(jnp.float32)).astype(jnp.bfloat16)
        all_differ = lax.all_gather(differ, "tp", axis=0, tiled=True)
        grouped = all_differ.reshape(4, group_width, rows_dev)
        mixed_all = jnp.einsum(
            "gcd,gct->gdt", group_mix[layer_idx], grouped, preferred_element_type=jnp.float32
        ).reshape(pool_width, rows_dev)
        mixed_all = (mixed_all * pool_gain[layer_idx][:, None]).astype(jnp.bfloat16)
        branch = lax.dot_general(
            mixed_all, out_block, (((0,), (0,)), ((), ())), preferred_element_type=jnp.float32
        )
        resid = residual_scale * stream.astype(jnp.float32) + branch
        row_sums, squares = lax.psum((jnp.sum(resid, axis=1), jnp.sum(resid * resid, axis=1)), "tp")
        row_mean = row_sums / model_width
        row_var = squares / model_width - row_mean * row_mean
        normed = (resid - row_mean[:, None]) * lax.rsqrt(row_var[:, None] + norm_eps)
        stream = (normed * norm_gain[layer_idx][None, :] + norm_bias[layer_idx][None, :]).astype(
            jnp.bfloat16
        )
    return stream


def solution(mesh):
    in_specs = (
        P("sp", "tp"),
        P(None, "tp", "sp"),
        P(),
        P(),
        P(None, "sp", "tp"),
        P(None, "tp"),
        P(None, "tp"),
    )
    out_specs = P("sp", "tp")
    return jax.shard_map(
        on_device, mesh=mesh, in_specs=in_specs, out_specs=out_specs, check_vma=False
    )
```

profile of v0, /device:TPU:0, one launch (start us, length us, event | category | flops | bytes accessed | tf_op | source)
XLA Modules:
  0.0 468.3 jit_solution(7111326799867742258)
XLA Ops:
  7.3 104.3 %all-gather.6.cloned.1.call-done = bf16[3,1024,1024]{2,1,0:T(8,128)(2,1)} async-done(((bf16[3,1024,128]{2,1,0:T(8,128)(2,1)}), bf16[3,1024,1024]{2,1,0:T(8,128)(2,1)}) %all-gather.6.cloned.1.call-update) | async-done | bytes 6291472 | tf_op jit(solution)/shard_map/all_gather | solution.py:37
  111.6 5.0 %fusion.6 = bf16[1024,768]{1,0:T(8,128)(2,1)} fusion(bf16[768,1024]{1,0:T(8,128)(2,1)} %param.7, bf16[3,1024,1024]{2,1,0:T(8,128)(2,1)} %all-gather.6.cloned.1.call-done), kind=kOutput, calls=%fused_computation.24 | convolution fusion | flops 1611399168 | bytes 5242880 | tf_op jit(solution)/shard_map/dot_general | solution.py:45
  116.8 26.3 %reduce-scatter.4.cloned.1.call-done = bf16[256,768]{1,0:T(8,128)(2,1)} async-done(((bf16[1024,768]{1,0:T(8,128)(2,1)}), bf16[256,768]{1,0:T(8,128)(2,1)}) %reduce-scatter.4.cloned.1.call-update) | async-done | bytes 393232 | tf_op jit(solution)/shard_map/reduce_scatter | solution.py:44
  144.0 3.4 collective-permute-start
  147.4 1.3 collective-permute-start.1
  149.3 4.3 collective-permute-done.1
  154.8 5.1 %fusion.44 = bf16[256,768]{1,0:T(8,128)(2,1)} fusion(bf16[256,768]{1,0:T(8,128)(2,1)} %reduce-scatter.4.cloned.1.call-done, f32[256,784]{1,0:T(8,128)S(1)} %maximum_convert_fusion, f32[768]{0:T(1024)S(1)} %get-tuple-element.41, f32[768]{0:T(1024)S(1)} %get-tuple-element.42, f32[768]{0:T(1024)S(1)} %get-tuple-element.43, f32[768]{0:T(1024)S(1)} %get-tuple-element.44, ...), kind=kLoop, calls=%fused_computation.83 | loop fusion | flops 7274496 | bytes 13382656 | tf_op jit(solution)/shard_map/convert_element_type | solution.py:71
  160.7 19.0 %all-gather.8.cloned.1.call-done = bf16[1024,768]{1,0:T(8,128)(2,1)} async-done(((bf16[256,768]{1,0:T(8,128)(2,1)}), bf16[1024,768]{1,0:T(8,128)(2,1)}) %all-gather.8.cloned.1.call-update) | async-done | bytes 1572880 | tf_op jit(solution)/shard_map/all_gather | solution.py:72
  179.7 2.0 multiply_convert_fusion.2
  181.7 98.7 %all-gather.10.cloned.1.call-done = bf16[3,1024,1024]{2,1,0:T(8,128)(2,1)} async-done(((bf16[3,128,1024]{2,1,0:T(8,128)(2,1)}), bf16[3,1024,1024]{2,1,0:T(8,128)(2,1)}) %all-gather.10.cloned.1.call-update) | async-done | bytes 6291472 | tf_op jit(solution)/shard_map/all_gather | solution.py:38
  280.5 5.8 %fusion.55 = (f32[768]{0:T(1024)S(1)}, f32[768]{0:T(1024)S(1)}, f32[768,1024]{1,0:T(8,128)}) fusion(bf16[1024,768]{1,0:T(8,128)(2,1)S(1)} %bitcast.86, bf16[3,1024,1024]{2,1,0:T(8,128)(2,1)} %all-gather.10.cloned.1.call-done, bf16[768,1024]{1,0:T(8,128)(2,1)} %param.7), kind=kOutput, calls=%fused_computation.119 | convolution fusion | flops 1615329792 | bytes 8394752 | tf_op jit(solution)/shard_map/dot_general | solution.py:78
  286.2 5.7 %all-reduce.2 = (f32[768]{0:T(1024)S(1)}, f32[768]{0:T(1024)S(1)}) all-reduce(f32[768]{0:T(1024)S(1)} %get-tuple-element.10, f32[768]{0:T(1024)S(1)} %get-tuple-element.9), channel_id=1, replica_groups=mesh['sp'=8,'tp'=4] {'tp'}, use_global_device_ids=true, to_apply=%region_4.5 | all-reduce | flops 1536 | bytes 12288 | tf_op jit(solution)/shard_map/psum | solution.py:82
  292.0 5.9 %fusion.10 = bf16[1024,768]{1,0:T(8,128)(2,1)} fusion(bf16[3,1024,1024]{2,1,0:T(8,128)(2,1)} %all-gather.6.cloned.1.call-done, f32[768,1024]{1,0:T(8,128)} %get-tuple-element.38, f32[1024]{0:T(1024)S(1)} %bitcast.95, f32[1024]{0:T(1024)S(1)} %bitcast.93, f32[768]{0:T(1024)S(1)} %get-tuple-element.37, f32[768]{0:T(1024)S(1)} %get-tuple-element.36), kind=kOutput, calls=%fused_computation.28 | convolution fusion | flops 1615331328 | bytes 6830080 | tf_op jit(solution)/shard_map/dot_general | solution.py:45
  298.0 26.6 %reduce-scatter.6.cloned.1.call-done = bf16[256,768]{1,0:T(8,128)(2,1)} async-done(((bf16[1024,768]{1,0:T(8,128)(2,1)}), bf16[256,768]{1,0:T(8,128)(2,1)}) %reduce-scatter.6.cloned.1.call-update) | async-done | bytes 393232 | tf_op jit(solution)/shard_map/reduce_scatter | solution.py:44
  325.6 3.4 collective-permute-start.2
  328.9 1.3 collective-permute-start.3
  330.8 4.3 collective-permute-done.3
  336.3 5.0 %fusion.45 = bf16[256,768]{1,0:T(8,128)(2,1)} fusion(bf16[256,768]{1,0:T(8,128)(2,1)} %reduce-scatter.6.cloned.1.call-done, f32[256,784]{1,0:T(8,128)S(1)} %maximum_convert_fusion.1, f32[768]{0:T(1024)S(1)} %get-tuple-element.41, f32[768]{0:T(1024)S(1)} %get-tuple-element.42, f32[768]{0:T(1024)S(1)} %get-tuple-element.43, f32[768]{0:T(1024)S(1)} %get-tuple-element.44, ...), kind=kLoop, calls=%fused_computation.84 | loop fusion | flops 7274496 | bytes 13382656 | tf_op jit(solution)/shard_map/convert_element_type | solution.py:71
  341.5 19.5 %all-gather.12.cloned.1.call-done = bf16[1024,768]{1,0:T(8,128)(2,1)} async-done(((bf16[256,768]{1,0:T(8,128)(2,1)}), bf16[1024,768]{1,0:T(8,128)(2,1)}) %all-gather.12.cloned.1.call-update) | async-done | bytes 1572880 | tf_op jit(solution)/shard_map/all_gather | solution.py:72
  361.1 2.2 multiply_convert_fusion.1
  363.5 5.9 %fusion.54 = (f32[768]{0:T(1024)S(1)}, f32[768]{0:T(1024)S(1)}, f32[768,1024]{1,0:T(8,128)}) fusion(bf16[1024,768]{1,0:T(8,128)(2,1)S(1)} %bitcast.85, bf16[3,1024,1024]{2,1,0:T(8,128)(2,1)} %all-gather.10.cloned.1.call-done, f32[1024]{0:T(1024)S(1)} %bitcast.96, f32[1024]{0:T(1024)S(1)} %bitcast.94, f32[768]{0:T(1024)S(1)} %get-tuple-element.37, ...), kind=kOutput, calls=%fused_computation.118 | convolution fusion | flops 1619261952 | bytes 9981952 | tf_op jit(solution)/shard_map/dot_general | solution.py:78
  369.3 6.0 %all-reduce.1 = (f32[768]{0:T(1024)S(1)}, f32[768]{0:T(1024)S(1)}) all-reduce(f32[768]{0:T(1024)S(1)} %get-tuple-element.8, f32[768]{0:T(1024)S(1)} %get-tuple-element.7), channel_id=1, replica_groups=mesh['sp'=8,'tp'=4] {'tp'}, use_global_device_ids=true, to_apply=%region_9.10 | all-reduce | flops 1536 | bytes 12288 | tf_op jit(solution)/shard_map/psum | solution.py:82
  375.3 5.9 %fusion.9 = bf16[1024,768]{1,0:T(8,128)(2,1)} fusion(bf16[3,1024,1024]{2,1,0:T(8,128)(2,1)} %all-gather.6.cloned.1.call-done, f32[768,1024]{1,0:T(8,128)} %get-tuple-element.39, f32[1024]{0:T(1024)S(1)} %bitcast.91, f32[1024]{0:T(1024)S(1)} %bitcast.89, f32[768]{0:T(1024)S(1)} %get-tuple-element.35, f32[768]{0:T(1024)S(1)} %get-tuple-element.34), kind=kOutput, calls=%fused_computation.27 | convolution fusion | flops 1615331328 | bytes 6830080 | tf_op jit(solution)/shard_map/dot_general | solution.py:45
  381.3 29.2 %reduce-scatter.8.cloned.1.call-done = bf16[256,768]{1,0:T(8,128)(2,1)} async-done(((bf16[1024,768]{1,0:T(8,128)(2,1)}), bf16[256,768]{1,0:T(8,128)(2,1)}) %reduce-scatter.8.cloned.1.call-update) | async-done | bytes 393232 | tf_op jit(solution)/shard_map/reduce_scatter | solution.py:44
  411.5 3.4 collective-permute-start.4
  416.7 4.3 collective-permute-done.5
  422.2 5.0 %fusion.46 = bf16[256,768]{1,0:T(8,128)(2,1)} fusion(bf16[256,768]{1,0:T(8,128)(2,1)} %reduce-scatter.8.cloned.1.call-done, f32[256,784]{1,0:T(8,128)S(1)} %maximum_convert_fusion.2, f32[768]{0:T(1024)S(1)} %get-tuple-element.41, f32[768]{0:T(1024)S(1)} %get-tuple-element.42, f32[768]{0:T(1024)S(1)} %get-tuple-element.43, f32[768]{0:T(1024)S(1)} %get-tuple-element.44, ...), kind=kLoop, calls=%fused_computation.85 | loop fusion | flops 7274496 | bytes 13382656 | tf_op jit(solution)/shard_map/convert_element_type | solution.py:71
  427.2 19.8 %all-gather.14.cloned.1.call-done = bf16[1024,768]{1,0:T(8,128)(2,1)} async-done(((bf16[256,768]{1,0:T(8,128)(2,1)}), bf16[1024,768]{1,0:T(8,128)(2,1)}) %all-gather.14.cloned.1.call-update) | async-done | bytes 1572880 | tf_op jit(solution)/shard_map/all_gather | solution.py:72
  447.0 2.2 multiply_convert_fusion
  449.4 4.4 fusion.53
  453.7 6.0 %all-reduce = (f32[768]{0:T(1024)S(1)}, f32[768]{0:T(1024)S(1)}) all-reduce(f32[768]{0:T(1024)S(1)} %get-tuple-element.6, f32[768]{0:T(1024)S(1)} %get-tuple-element.5), channel_id=1, replica_groups=mesh['sp'=8,'tp'=4] {'tp'}, use_global_device_ids=true, to_apply=%region_14.15 | all-reduce | flops 1536 | bytes 12288 | tf_op jit(solution)/shard_map/psum | solution.py:82
  459.7 1.7 add_convert_fusion
  (51 shorter events, 11.9 us)
Async XLA Ops:
  6.5 105.1 %all-gather.6.cloned.1.call-start = ((), (), s32[]{:S(2)}) async-start(), calls=%async_computation.3 | async-start | bytes 7077888 | tf_op jit(solution)/shard_map/all_gather | solution.py:37
  7.3 135.8 %reduce-scatter.4.cloned.1.call-start = ((), (), s32[]{:S(2)}) async-start(), calls=%async_computation.4 | async-start | bytes 1966080 | tf_op jit(solution)/shard_map/reduce_scatter | solution.py:44
  116.7 63.0 %all-gather.8.cloned.1.call-start = ((), (), s32[]{:S(2)}) async-start(), calls=%async_computation.5 | async-start | bytes 1966080 | tf_op jit(solution)/shard_map/all_gather | solution.py:72
  144.0 5.3 %collective-permute-start = (bf16[256,8]{1,0:T(8,128)(2,1)S(1)}, bf16[256,8]{1,0:T(8,128)(2,1)S(1)}, u32[]{:S(2)}, u32[]{:S(2)}) collective-permute-start(bf16[256,8]{1,0:T(8,128)(2,1)S(1)} %get-tuple-element.24), channel_id=1, source_target_pairs={{0,4},{4,8},{8,12},{12,16},{16,20},{20,24},{24,28},{1,5},{5,9},{9,... | collective-permute-start | bytes 12296 | tf_op jit(solution)/shard_map/ppermute | solution.py:17
  147.4 6.2 %collective-permute-start.1 = (bf16[256,8]{1,0:T(8,128)(2,1)S(1)}, bf16[256,8]{1,0:T(8,128)(2,1)S(1)}, u32[]{:S(2)}, u32[]{:S(2)}) collective-permute-start(bf16[256,8]{1,0:T(8,128)(2,1)S(1)} %get-tuple-element.25), channel_id=1, source_target_pairs={{4,0},{8,4},{12,8},{16,12},{20,16},{24,20},{28,24},{5,1},{9,5},{13... | collective-permute-start | bytes 12296 | tf_op jit(solution)/shard_map/ppermute | solution.py:18
  154.8 5.8 %copy-start.1 = (f32[3,1024]{1,0:T(4,128)S(1)}, f32[3,1024]{1,0:T(4,128)}, u32[]{:S(2)}) copy-start(f32[3,1024]{1,0:T(4,128)} %param.10) | copy-start | bytes 36868
  154.8 5.8 %copy-start.2 = (f32[3,1024]{1,0:T(4,128)S(1)}, f32[3,1024]{1,0:T(4,128)}, u32[]{:S(2)}) copy-start(f32[3,1024]{1,0:T(4,128)} %param.12) | copy-start | bytes 36868
  154.8 5.8 %copy-start.3 = (f32[3,1024]{1,0:T(4,128)S(1)}, f32[3,1024]{1,0:T(4,128)}, u32[]{:S(2)}) copy-start(f32[3,1024]{1,0:T(4,128)} %param.13) | copy-start | bytes 36868
  154.8 24.9 %copy-start = (bf16[3,4,256,256]{3,2,1,0:T(8,128)(2,1)S(1)}, bf16[3,4,256,256]{3,2,1,0:T(8,128)(2,1)}, u32[]{:S(2)}) copy-start(bf16[3,4,256,256]{3,2,1,0:T(8,128)(2,1)} %param.9) | copy-start | bytes 4718596
  159.9 120.5 %all-gather.10.cloned.1.call-start = ((), (), s32[]{:S(2)}) async-start(), calls=%async_computation.6 | async-start | bytes 7077888 | tf_op jit(solution)/shard_map/all_gather | solution.py:38
  160.5 164.1 %reduce-scatter.6.cloned.1.call-start = ((), (), s32[]{:S(2)}) async-start(), calls=%async_computation.7 | async-start | bytes 1966080 | tf_op jit(solution)/shard_map/reduce_scatter | solution.py:44
  297.9 63.2 %all-gather.12.cloned.1.call-start = ((), (), s32[]{:S(2)}) async-start(), calls=%async_computation.8 | async-start | bytes 1966080 | tf_op jit(solution)/shard_map/all_gather | solution.py:72
  325.6 5.3 %collective-permute-start.2 = (bf16[256,8]{1,0:T(8,128)(2,1)S(1)}, bf16[256,8]{1,0:T(8,128)(2,1)S(1)}, u32[]{:S(2)}, u32[]{:S(2)}) collective-permute-start(bf16[256,8]{1,0:T(8,128)(2,1)S(1)} %get-tuple-element.22), channel_id=1, source_target_pairs={{0,4},{4,8},{8,12},{12,16},{16,20},{20,24},{24,28},{1,5},{5,9},{9,... | collective-permute-start | bytes 12296 | tf_op jit(solution)/shard_map/ppermute | solution.py:17
  328.9 6.2 %collective-permute-start.3 = (bf16[256,8]{1,0:T(8,128)(2,1)S(1)}, bf16[256,8]{1,0:T(8,128)(2,1)S(1)}, u32[]{:S(2)}, u32[]{:S(2)}) collective-permute-start(bf16[256,8]{1,0:T(8,128)(2,1)S(1)} %get-tuple-element.23), channel_id=1, source_target_pairs={{4,0},{8,4},{12,8},{16,12},{20,16},{24,20},{28,24},{5,1},{9,5},{13... | collective-permute-start | bytes 12296 | tf_op jit(solution)/shard_map/ppermute | solution.py:18
  341.3 69.2 %reduce-scatter.8.cloned.1.call-start = ((), (), s32[]{:S(2)}) async-start(), calls=%async_computation.9 | async-start | bytes 1966080 | tf_op jit(solution)/shard_map/reduce_scatter | solution.py:44
  361.1 2.4 copy-start.4
  381.2 65.8 %all-gather.14.cloned.1.call-start = ((), (), s32[]{:S(2)}) async-start(), calls=%async_computation.10 | async-start | bytes 1966080 | tf_op jit(solution)/shard_map/all_gather | solution.py:72
  411.5 5.3 %collective-permute-start.4 = (bf16[256,8]{1,0:T(8,128)(2,1)S(1)}, bf16[256,8]{1,0:T(8,128)(2,1)S(1)}, u32[]{:S(2)}, u32[]{:S(2)}) collective-permute-start(bf16[256,8]{1,0:T(8,128)(2,1)S(1)} %get-tuple-element.20), channel_id=1, source_target_pairs={{0,4},{4,8},{8,12},{12,16},{16,20},{20,24},{24,28},{1,5},{5,9},{9,... | collective-permute-start | bytes 12296 | tf_op jit(solution)/shard_map/ppermute | solution.py:17
  414.8 6.2 %collective-permute-start.5 = (bf16[256,8]{1,0:T(8,128)(2,1)S(1)}, bf16[256,8]{1,0:T(8,128)(2,1)S(1)}, u32[]{:S(2)}, u32[]{:S(2)}) collective-permute-start(bf16[256,8]{1,0:T(8,128)(2,1)S(1)} %get-tuple-element.21), channel_id=1, source_target_pairs={{4,0},{8,4},{12,8},{16,12},{20,16},{24,20},{28,24},{5,1},{9,5},{13... | collective-permute-start | bytes 12296 | tf_op jit(solution)/shard_map/ppermute | solution.py:18
  447.0 2.4 copy-start.5
Sparse Core Ops, SparseCore 0:
  9.4 102.1 all-gather.5
  116.8 26.2 reduce-scatter.3
  160.1 19.5 all-gather.7
  181.7 98.6 all-gather.9
  298.0 26.4 reduce-scatter.5
  341.4 19.6 all-gather.11
  381.3 29.1 reduce-scatter.7
  427.3 19.6 all-gather.13
where the time goes:
time: 469 us; the launch traced here: 468 us
  waiting for transfers between devices  359 us (77%)
  matrix products  39.2 us (8%)
  other arithmetic  20.4 us (4%)
  blocking collectives  17.7 us (4%)
  starting transfers between devices  14.5 us (3%)
  between operations  13.8 us (3%)
    all_gather x1, waiting for transfers between devices, on_device(): lax.all_gather(in_proj, 'sp', axis=2, tiled=True)  104 us
    all_gather x1, waiting for transfers between devices, on_device(): lax.all_gather(out_proj, 'sp', axis=1, tiled=True)  98.7 us
    reduce_scatter x3, waiting for transfers between devices, on_device(): lax.psum_scatter(lax.dot_general(in_block, stream, (((0,), (1,)), ((), ()...  82.1 us
    all_gather x3, waiting for transfers between devices, on_device(): all_differ = lax.all_gather(differ, 'tp', axis=0, tiled=True)  58.3 us
    psum x3, blocking collectives, on_device(): lax.psum((jnp.sum(resid, axis=1), jnp.sum(resid * resid, axis=1)), 'tp')  17.7 us
    dot_general x3, matrix products, on_device(): lax.dot_general(in_block, stream, (((0,), (1,)), ((), ())), preferred_ele...  16.8 us
    dot_general x3, matrix products, on_device(): lax.dot_general(mixed_all, out_block, (((0,), (0,)), ((), ())), preferred...  16 us
    convert_element_type x3, other arithmetic, on_device(): differ = (pooled - projected.astype(jnp.float32)).astype(jnp.bfloat16)  15 us
  transfers between devices with their start and end apart: 14, of which 14 were waited for; matrix products, arithmetic and copies ran while one was open for 0% of the time, Pallas kernels for 0%

commit v1 on v0

--- a/solution.py
+++ b/solution.py
@@ -35,7 +35,7 @@
     chan_groups = (lax.axis_index("tp") * chan_share + jnp.arange(chan_share)) // group_width
     in_all, out_all = (
         lax.all_gather(in_proj, "sp", axis=2, tiled=True),
-        lax.all_gather(out_proj, "sp", axis=1, tiled=True),
+        jnp.concatenate(lax.all_gather(out_proj, "sp"), axis=1),
     )
     stream = tokens
     for layer_idx in range(layer_count):

time: 469 us -> 455 us (0.970)
  waiting for transfers between devices: 359 us -> 341 us
  local copies, waits for them, and re-layouts: 3.32 us -> 9.37 us
    all_gather x1, waiting for transfers between devices: 98.7 us -> 84 us  [on_device(): lax.all_gather(out_proj, 'sp')]
    slice x0 -> x1, local copies, waits for them, and re-layouts: none -> 5.91 us  [on_device(): out_block = out_all[layer_idx]]
    all_gather x3, waiting for transfers between devices: 58.3 us -> 52.8 us  [on_device(): all_differ = lax.all_gather(differ, 'tp', axis=0, tiled=True)]
  transfers between devices with their start and end apart: 14 -> 14, of which waited for: 14 -> 14; matrix products, arithmetic and copies ran while one was open for 0% -> 3% of each run, Pallas kernels for 0% -> 0%
where the time goes in v1:
time: 455 us; the launch traced here: 454 us
  waiting for transfers between devices  341 us (75%)
  matrix products  37.2 us (8%)
  other arithmetic  20.3 us (4%)
  blocking collectives  17.9 us (4%)
  starting transfers between devices  14.7 us (3%)
  between operations  13.8 us (3%)
  local copies, waits for them, and re-layouts  9.37 us (2%)
    all_gather x1, waiting for transfers between devices, on_device(): lax.all_gather(in_proj, 'sp', axis=2, tiled=True)  104 us
    reduce_scatter x3, waiting for transfers between devices, on_device(): lax.psum_scatter(lax.dot_general(in_block, stream, (((0,), (1,)), ((), ()...  84 us
    all_gather x1, waiting for transfers between devices, on_device(): lax.all_gather(out_proj, 'sp')  84 us
    all_gather x3, waiting for transfers between devices, on_device(): all_differ = lax.all_gather(differ, 'tp', axis=0, tiled=True)  52.8 us
    psum x3, blocking collectives, on_device(): lax.psum((jnp.sum(resid, axis=1), jnp.sum(resid * resid, axis=1)), 'tp')  17.9 us
    dot_general x3, matrix products, on_device(): lax.dot_general(in_block, stream, (((0,), (1,)), ((), ())), preferred_ele...  16.8 us
    convert_element_type x3, other arithmetic, on_device(): differ = (pooled - projected.astype(jnp.float32)).astype(jnp.bfloat16)  14.9 us
    dot_general x3, matrix products, on_device(): lax.dot_general(mixed_all, out_block, (((0,), (0,)), ((), ())), preferred...  13.5 us
  transfers between devices with their start and end apart: 14, of which 14 were waited for; matrix products, arithmetic and copies ran while one was open for 3% of the time, Pallas kernels for 0%

profile of v1, /device:TPU:0, one launch (start us, length us, event | category | flops | bytes accessed | tf_op | source)
XLA Modules:
  0.0 454.0 jit_solution(15600836041073174516)
XLA Ops:
  7.3 104.3 %all-gather.7.cloned.1.call-done = bf16[3,1024,1024]{2,1,0:T(8,128)(2,1)} async-done(((bf16[3,1024,128]{2,1,0:T(8,128)(2,1)}), bf16[3,1024,1024]{2,1,0:T(8,128)(2,1)}) %all-gather.7.cloned.1.call-update) | async-done | bytes 6291472 | tf_op jit(solution)/shard_map/all_gather | solution.py:37
  111.6 5.0 %fusion.3 = bf16[1024,768]{1,0:T(8,128)(2,1)} fusion(bf16[768,1024]{1,0:T(8,128)(2,1)} %param.7, bf16[3,1024,1024]{2,1,0:T(8,128)(2,1)} %all-gather.7.cloned.1.call-done), kind=kOutput, calls=%fused_computation.18 | convolution fusion | flops 1611399168 | bytes 5242880 | tf_op jit(solution)/shard_map/dot_general | solution.py:45
  117.5 25.5 %reduce-scatter.4.cloned.1.call-done = bf16[256,768]{1,0:T(8,128)(2,1)} async-done(((bf16[1024,768]{1,0:T(8,128)(2,1)}), bf16[256,768]{1,0:T(8,128)(2,1)}) %reduce-scatter.4.cloned.1.call-update) | async-done | bytes 393232 | tf_op jit(solution)/shard_map/reduce_scatter | solution.py:44
  144.0 3.4 collective-permute-start
  149.3 4.3 collective-permute-done.1
  154.8 5.0 %fusion.41 = bf16[256,768]{1,0:T(8,128)(2,1)} fusion(bf16[256,768]{1,0:T(8,128)(2,1)} %reduce-scatter.4.cloned.1.call-done, f32[256,784]{1,0:T(8,128)S(1)} %maximum_convert_fusion, f32[768]{0:T(1024)S(1)} %get-tuple-element.44, f32[768]{0:T(1024)S(1)} %get-tuple-element.45, f32[768]{0:T(1024)S(1)} %get-tuple-element.46, f32[768]{0:T(1024)S(1)} %get-tuple-element.47, ...), kind=kLoop, calls=%fused_computation.77 | loop fusion | flops 7274496 | bytes 13382656 | tf_op jit(solution)/shard_map/convert_element_type | solution.py:71
  160.0 84.0 %all-gather.15.cloned.1.call-done = bf16[24,128,1024]{2,1,0:T(8,128)(2,1)} async-done(((bf16[3,128,1024]{2,1,0:T(8,128)(2,1)}), bf16[24,128,1024]{2,1,0:T(8,128)(2,1)}) %all-gather.15.cloned.1.call-update) | async-done | bytes 6291472 | tf_op jit(solution)/shard_map/all_gather | solution.py:38
  244.0 5.9 %fusion.53 = (bf16[1,8,128,1024]{3,2,0,1:T(8,128)(2,1)}, bf16[1,8,128,1024]{3,2,0,1:T(8,128)(2,1)S(1)}, bf16[1,8,128,1024]{3,2,0,1:T(8,128)(2,1)}) fusion(bf16[3,8,128,1024]{3,2,0,1:T(8,128)(2,1)} %bitcast.69), kind=kLoop, calls=%fused_computation.114 | loop fusion | bytes 12582912 | tf_op jit(solution)/shard_map/slice | solution.py:43
  249.9 13.3 %all-gather.9.cloned.1.call-done = bf16[1024,768]{1,0:T(8,128)(2,1)} async-done(((bf16[256,768]{1,0:T(8,128)(2,1)}), bf16[1024,768]{1,0:T(8,128)(2,1)}) %all-gather.9.cloned.1.call-update) | async-done | bytes 1572880 | tf_op jit(solution)/shard_map/all_gather | solution.py:72
  263.2 2.3 multiply_convert_fusion.2
  265.9 3.9 fusion.52
  269.8 6.0 %all-reduce.2 = (f32[768]{0:T(1024)S(1)}, f32[768]{0:T(1024)S(1)}) all-reduce(f32[768]{0:T(1024)S(1)} %get-tuple-element.10, f32[768]{0:T(1024)S(1)} %get-tuple-element.9), channel_id=1, replica_groups=mesh['sp'=8,'tp'=4] {'tp'}, use_global_device_ids=true, to_apply=%region_4.5 | all-reduce | flops 1536 | bytes 12288 | tf_op jit(solution)/shard_map/psum | solution.py:82
  275.8 5.9 %fusion.7 = bf16[1024,768]{1,0:T(8,128)(2,1)} fusion(bf16[3,1024,1024]{2,1,0:T(8,128)(2,1)} %all-gather.7.cloned.1.call-done, f32[768,1024]{1,0:T(8,128)} %get-tuple-element.41, f32[1024]{0:T(1024)S(1)} %bitcast.87, f32[1024]{0:T(1024)S(1)} %bitcast.85, f32[768]{0:T(1024)S(1)} %get-tuple-element.40, f32[768]{0:T(1024)S(1)} %get-tuple-element.39), kind=kOutput, calls=%fused_computation.22 | convolution fusion | flops 1615331328 | bytes 6830080 | tf_op jit(solution)/shard_map/dot_general | solution.py:45
  281.8 29.2 %reduce-scatter.6.cloned.1.call-done = bf16[256,768]{1,0:T(8,128)(2,1)} async-done(((bf16[1024,768]{1,0:T(8,128)(2,1)}), bf16[256,768]{1,0:T(8,128)(2,1)}) %reduce-scatter.6.cloned.1.call-update) | async-done | bytes 393232 | tf_op jit(solution)/shard_map/reduce_scatter | solution.py:44
  311.9 3.4 collective-permute-start.2
  317.2 4.3 collective-permute-done.3
  322.7 5.0 %fusion.42 = bf16[256,768]{1,0:T(8,128)(2,1)} fusion(bf16[256,768]{1,0:T(8,128)(2,1)} %reduce-scatter.6.cloned.1.call-done, f32[256,784]{1,0:T(8,128)S(1)} %maximum_convert_fusion.1, f32[768]{0:T(1024)S(1)} %get-tuple-element.44, f32[768]{0:T(1024)S(1)} %get-tuple-element.45, f32[768]{0:T(1024)S(1)} %get-tuple-element.46, f32[768]{0:T(1024)S(1)} %get-tuple-element.47, ...), kind=kLoop, calls=%fused_computation.78 | loop fusion | flops 7274496 | bytes 13382656 | tf_op jit(solution)/shard_map/convert_element_type | solution.py:71
  327.8 19.7 %all-gather.11.cloned.1.call-done = bf16[1024,768]{1,0:T(8,128)(2,1)} async-done(((bf16[256,768]{1,0:T(8,128)(2,1)}), bf16[1024,768]{1,0:T(8,128)(2,1)}) %all-gather.11.cloned.1.call-update) | async-done | bytes 1572880 | tf_op jit(solution)/shard_map/all_gather | solution.py:72
  347.5 2.3 multiply_convert_fusion.1
  350.0 4.4 fusion.51
  354.4 6.0 %all-reduce.1 = (f32[768]{0:T(1024)S(1)}, f32[768]{0:T(1024)S(1)}) all-reduce(f32[768]{0:T(1024)S(1)} %get-tuple-element.8, f32[768]{0:T(1024)S(1)} %get-tuple-element.7), channel_id=1, replica_groups=mesh['sp'=8,'tp'=4] {'tp'}, use_global_device_ids=true, to_apply=%region_9.10 | all-reduce | flops 1536 | bytes 12288 | tf_op jit(solution)/shard_map/psum | solution.py:82
  360.3 5.9 %fusion.6 = bf16[1024,768]{1,0:T(8,128)(2,1)} fusion(bf16[3,1024,1024]{2,1,0:T(8,128)(2,1)} %all-gather.7.cloned.1.call-done, f32[768,1024]{1,0:T(8,128)} %get-tuple-element.42, f32[1024]{0:T(1024)S(1)} %bitcast.83, f32[1024]{0:T(1024)S(1)} %bitcast.81, f32[768]{0:T(1024)S(1)} %get-tuple-element.38, f32[768]{0:T(1024)S(1)} %get-tuple-element.37), kind=kOutput, calls=%fused_computation.21 | convolution fusion | flops 1615331328 | bytes 6830080 | tf_op jit(solution)/shard_map/dot_general | solution.py:45
  366.3 29.2 %reduce-scatter.8.cloned.1.call-done = bf16[256,768]{1,0:T(8,128)(2,1)} async-done(((bf16[1024,768]{1,0:T(8,128)(2,1)}), bf16[256,768]{1,0:T(8,128)(2,1)}) %reduce-scatter.8.cloned.1.call-update) | async-done | bytes 393232 | tf_op jit(solution)/shard_map/reduce_scatter | solution.py:44
  396.5 3.4 collective-permute-start.4
  399.9 1.5 collective-permute-start.5
  401.8 4.3 collective-permute-done.5
  407.3 5.0 %fusion.43 = bf16[256,768]{1,0:T(8,128)(2,1)} fusion(bf16[256,768]{1,0:T(8,128)(2,1)} %reduce-scatter.8.cloned.1.call-done, f32[256,784]{1,0:T(8,128)S(1)} %maximum_convert_fusion.2, f32[768]{0:T(1024)S(1)} %get-tuple-element.44, f32[768]{0:T(1024)S(1)} %get-tuple-element.45, f32[768]{0:T(1024)S(1)} %get-tuple-element.46, f32[768]{0:T(1024)S(1)} %get-tuple-element.47, ...), kind=kLoop, calls=%fused_computation.79 | loop fusion | flops 7274496 | bytes 13382656 | tf_op jit(solution)/shard_map/convert_element_type | solution.py:71
  412.2 19.8 %all-gather.13.cloned.1.call-done = bf16[1024,768]{1,0:T(8,128)(2,1)} async-done(((bf16[256,768]{1,0:T(8,128)(2,1)}), bf16[1024,768]{1,0:T(8,128)(2,1)}) %all-gather.13.cloned.1.call-update) | async-done | bytes 1572880 | tf_op jit(solution)/shard_map/all_gather | solution.py:72
  432.0 2.2 multiply_convert_fusion
  434.2 5.2 %fusion.50 = (f32[768]{0:T(1024)S(1)}, f32[768]{0:T(1024)S(1)}, f32[768,1024]{1,0:T(8,128)S(1)}) fusion(bf16[1024,768]{1,0:T(8,128)(2,1)S(1)} %bitcast.75, bf16[1024,1024]{1,0:T(8,128)(2,1)} %bitcast.70, f32[1024]{0:T(1024)S(1)} %bitcast.84, f32[1024]{0:T(1024)S(1)} %bitcast.82, f32[768]{0:T(1024)S(1)} %get-tuple-element.38, ...), kind=kOutput, calls=%fused_computation.111 | convolution fusion | flops 1619261952 | bytes 9981952 | tf_op jit(solution)/shard_map/dot_general | solution.py:78
  439.4 6.0 %all-reduce = (f32[768]{0:T(1024)S(1)}, f32[768]{0:T(1024)S(1)}) all-reduce(f32[768]{0:T(1024)S(1)} %get-tuple-element.6, f32[768]{0:T(1024)S(1)} %get-tuple-element.5), channel_id=1, replica_groups=mesh['sp'=8,'tp'=4] {'tp'}, use_global_device_ids=true, to_apply=%region_14.15 | all-reduce | flops 1536 | bytes 12288 | tf_op jit(solution)/shard_map/psum | solution.py:82
  445.4 1.7 add_convert_fusion
  (52 shorter events, 13.0 us)
Async XLA Ops:
  6.5 105.1 %all-gather.7.cloned.1.call-start = ((), (), s32[]{:S(2)}) async-start(), calls=%async_computation.3 | async-start | bytes 7077888 | tf_op jit(solution)/shard_map/all_gather | solution.py:37
  7.3 135.8 %reduce-scatter.4.cloned.1.call-start = ((), (), s32[]{:S(2)}) async-start(), calls=%async_computation.4 | async-start | bytes 1966080 | tf_op jit(solution)/shard_map/reduce_scatter | solution.py:44
  116.7 127.3 %all-gather.15.cloned.1.call-start = ((), (), s32[]{:S(2)}) async-start(), calls=%async_computation.10 | async-start | bytes 7077888 | tf_op jit(solution)/shard_map/all_gather | solution.py:38
  117.4 145.8 %all-gather.9.cloned.1.call-start = ((), (), s32[]{:S(2)}) async-start(), calls=%async_computation.5 | async-start | bytes 1966080 | tf_op jit(solution)/shard_map/all_gather | solution.py:72
  144.0 5.3 %collective-permute-start = (bf16[256,8]{1,0:T(8,128)(2,1)S(1)}, bf16[256,8]{1,0:T(8,128)(2,1)S(1)}, u32[]{:S(2)}, u32[]{:S(2)}) collective-permute-start(bf16[256,8]{1,0:T(8,128)(2,1)S(1)} %get-tuple-element.27), channel_id=1, source_target_pairs={{0,4},{4,8},{8,12},{12,16},{16,20},{20,24},{24,28},{1,5},{5,9},{9,... | collective-permute-start | bytes 12296 | tf_op jit(solution)/shard_map/ppermute | solution.py:17
  147.4 6.2 %collective-permute-start.1 = (bf16[256,8]{1,0:T(8,128)(2,1)S(1)}, bf16[256,8]{1,0:T(8,128)(2,1)S(1)}, u32[]{:S(2)}, u32[]{:S(2)}) collective-permute-start(bf16[256,8]{1,0:T(8,128)(2,1)S(1)} %get-tuple-element.28), channel_id=1, source_target_pairs={{4,0},{8,4},{12,8},{16,12},{20,16},{24,20},{28,24},{5,1},{9,5},{13... | collective-permute-start | bytes 12296 | tf_op jit(solution)/shard_map/ppermute | solution.py:18
  154.8 5.1 %copy-start.1 = (f32[3,1024]{1,0:T(4,128)S(1)}, f32[3,1024]{1,0:T(4,128)}, u32[]{:S(2)}) copy-start(f32[3,1024]{1,0:T(4,128)} %param.10) | copy-start | bytes 36868
  154.8 5.1 %copy-start.2 = (f32[3,1024]{1,0:T(4,128)S(1)}, f32[3,1024]{1,0:T(4,128)}, u32[]{:S(2)}) copy-start(f32[3,1024]{1,0:T(4,128)} %param.12) | copy-start | bytes 36868
  154.8 5.1 %copy-start.3 = (f32[3,1024]{1,0:T(4,128)S(1)}, f32[3,1024]{1,0:T(4,128)}, u32[]{:S(2)}) copy-start(f32[3,1024]{1,0:T(4,128)} %param.13) | copy-start | bytes 36868
  159.8 151.2 %reduce-scatter.6.cloned.1.call-start = ((), (), s32[]{:S(2)}) async-start(), calls=%async_computation.6 | async-start | bytes 1966080 | tf_op jit(solution)/shard_map/reduce_scatter | solution.py:44
  263.2 2.4 copy-start
  263.2 2.7 copy-start.4
  281.7 65.7 %all-gather.11.cloned.1.call-start = ((), (), s32[]{:S(2)}) async-start(), calls=%async_computation.7 | async-start | bytes 1966080 | tf_op jit(solution)/shard_map/all_gather | solution.py:72
  311.9 5.3 %collective-permute-start.2 = (bf16[256,8]{1,0:T(8,128)(2,1)S(1)}, bf16[256,8]{1,0:T(8,128)(2,1)S(1)}, u32[]{:S(2)}, u32[]{:S(2)}) collective-permute-start(bf16[256,8]{1,0:T(8,128)(2,1)S(1)} %get-tuple-element.25), channel_id=1, source_target_pairs={{0,4},{4,8},{8,12},{12,16},{16,20},{20,24},{24,28},{1,5},{5,9},{9,... | collective-permute-start | bytes 12296 | tf_op jit(solution)/shard_map/ppermute | solution.py:17
  315.3 6.2 %collective-permute-start.3 = (bf16[256,8]{1,0:T(8,128)(2,1)S(1)}, bf16[256,8]{1,0:T(8,128)(2,1)S(1)}, u32[]{:S(2)}, u32[]{:S(2)}) collective-permute-start(bf16[256,8]{1,0:T(8,128)(2,1)S(1)} %get-tuple-element.26), channel_id=1, source_target_pairs={{4,0},{8,4},{12,8},{16,12},{20,16},{24,20},{28,24},{5,1},{9,5},{13... | collective-permute-start | bytes 12296 | tf_op jit(solution)/shard_map/ppermute | solution.py:18
  327.7 67.8 %reduce-scatter.8.cloned.1.call-start = ((), (), s32[]{:S(2)}) async-start(), calls=%async_computation.8 | async-start | bytes 1966080 | tf_op jit(solution)/shard_map/reduce_scatter | solution.py:44
  347.5 2.5 copy-start.5
  366.3 65.7 %all-gather.13.cloned.1.call-start = ((), (), s32[]{:S(2)}) async-start(), calls=%async_computation.9 | async-start | bytes 1966080 | tf_op jit(solution)/shard_map/all_gather | solution.py:72
  396.5 5.3 %collective-permute-start.4 = (bf16[256,8]{1,0:T(8,128)(2,1)S(1)}, bf16[256,8]{1,0:T(8,128)(2,1)S(1)}, u32[]{:S(2)}, u32[]{:S(2)}) collective-permute-start(bf16[256,8]{1,0:T(8,128)(2,1)S(1)} %get-tuple-element.23), channel_id=1, source_target_pairs={{0,4},{4,8},{8,12},{12,16},{16,20},{20,24},{24,28},{1,5},{5,9},{9,... | collective-permute-start | bytes 12296 | tf_op jit(solution)/shard_map/ppermute | solution.py:17
  399.9 6.2 %collective-permute-start.5 = (bf16[256,8]{1,0:T(8,128)(2,1)S(1)}, bf16[256,8]{1,0:T(8,128)(2,1)S(1)}, u32[]{:S(2)}, u32[]{:S(2)}) collective-permute-start(bf16[256,8]{1,0:T(8,128)(2,1)S(1)} %get-tuple-element.24), channel_id=1, source_target_pairs={{4,0},{8,4},{12,8},{16,12},{20,16},{24,20},{28,24},{5,1},{9,5},{13... | collective-permute-start | bytes 12296 | tf_op jit(solution)/shard_map/ppermute | solution.py:18
Sparse Core Ops, SparseCore 0:
  9.4 102.1 all-gather.6
  116.8 26.2 reduce-scatter.3
  145.2 98.6 all-gather.14
  245.4 17.7 all-gather.8
  281.8 29.1 reduce-scatter.5
  327.8 19.5 all-gather.10
  366.4 29.1 reduce-scatter.7
  412.4 19.6 all-gather.12
